TPU v7x, 32 devices: a whole 2x2x4 slice. The times are simulated.
32 devices in a mesh: ep: 8 (over z, y), tp: 4 (over x, core).
Axes of the slice: x: 2, y: 2, z: 4, core: 2. Of those that a mesh axis runs over, the one named last changes fastest.
Arguments:
- tokens: bfloat16 [4096, 2048], P(('ep', 'tp')), may hold values from -6 to 6
- norm_gain: float32 [2048], replicated, may hold values from 0.1 to 1.9
- w_gate: bfloat16 [32, 2048, 512], P(('ep', 'tp')), may hold values from -0.125 to 0.125
- w_up: bfloat16 [32, 2048, 512], P(('ep', 'tp')), may hold values from -0.125 to 0.125
- w_down: bfloat16 [32, 512, 2048], P(('ep', 'tp')), may hold values from -0.25 to 0.25
- routing: int32 [4096, 2], P(('ep', 'tp')), may hold values from 0 to 31, as said below
- gate_weight: float32 [4096, 2], P(('ep', 'tp')), may hold values from 0.05 to 1
Outputs:
- combined: bfloat16 [4096, 2048], P(('ep', 'tp'))
Inputs may be any that keep to these rules, and one draw needn't show every extreme that they name: `routing`: A token's 2 experts are distinct and lie in one group of 4 consecutive experts. Of the 128 tokens of each device exactly 16 choose each group; no expert is named by more than 16 tokens of one device, and in every group one expert is named by exactly 16 tokens of every device.
All inputs are finite; a program needn't handle non-finite values.
Results may differ from a plain program's by a relative error of at most 0.0085.
Values may be sent and summed in bfloat16 or wider, within the bound.
A program may use at most 64 MiB of HBM per device.

v0:
```python
import functools
import jax
import jax.numpy as jnp
from jax import lax
from jax.experimental import pallas as pl
from jax.experimental.pallas import tpu as pltpu
from jax.sharding import PartitionSpec as P

BF = jnp.bfloat16
F32 = jnp.float32
MESH = pl.DeviceIdType.MESH


def flip(index, bits):
    unit = 1
    while unit <= bits:
        if bits & unit:
            index = index + unit - 2 * unit * lax.rem(lax.div(index, unit), 2)
        unit *= 2
    return index


def kernel(
    ep_count, tp_count, block, chunks,
    tok_ref, gain_ref, route_ref, gate_ref, wg_hbm, wu_hbm, wd_hbm, out_ref,
    wg, wu, wd, xcat, pack, rows_in, hid, part, pair_in, cross_out, cross_in, done, back,
    w_sem, disp_s, disp_r, core_s, core_r, x_s, x_r, fwd_s, fwd_r,
    pair_s, pair_r, cross_s, cross_r, ret_s, ret_r,
):
    toks, width = tok_ref.shape
    ff = wg.shape[1]
    slots = ep_count * block
    per = ep_count // chunks
    seg = per * block
    me_e = lax.axis_index("ep")
    me_t = lax.axis_index("tp")
    partner = {"tp": flip(me_t, 1)}
    across = {"tp": flip(me_t, 2)}
    peer = [{"ep": flip(me_e, d)} for d in range(ep_count)]

    w_copies = [
        pltpu.make_async_copy(src.at[0], dst, w_sem.at[i])
        for i, (src, dst) in enumerate(((wg_hbm, wg), (wu_hbm, wu), (wd_hbm, wd)))
    ]
    for c in w_copies:
        c.start()
    barrier = pltpu.get_barrier_semaphore()
    others = peer[1:] + [partner, across]
    for dev in others:
        pl.semaphore_signal(barrier, inc=1, device_id=dev, device_id_type=MESH)

    values = tok_ref[...].astype(F32)
    scale = lax.rsqrt(jnp.mean(values * values, axis=-1, keepdims=True) + 1e-06)
    xcat[:, :width] = (values * scale * gain_ref[...]).astype(BF)
    lane = lax.broadcasted_iota(jnp.int32, (toks, 128), 1)
    weight = jnp.zeros((toks, 128), F32)
    for k in range(route_ref.shape[1]):
        member = jnp.bitwise_and(route_ref[:, k : k + 1], tp_count - 1)
        hit = member == jnp.bitwise_and(lane, tp_count - 1)
        weight = weight + jnp.where(hit, gate_ref[:, k : k + 1], 0.0)
    hi = weight.astype(BF).astype(F32)
    mid = (weight - hi).astype(BF).astype(F32)
    low = weight - hi - mid
    tail = jnp.where(lane < tp_count, hi, jnp.where(lane < 2 * tp_count, mid, low))
    xcat[:, width:] = jnp.where(lane < 3 * tp_count, tail, 0.0).astype(BF)

    shift = tp_count.bit_length() - 1
    group = jnp.bitwise_xor(jnp.right_shift(route_ref[:, 0:1], shift), me_e)
    in_group = (group == lane).astype(F32)
    below = lax.broadcasted_iota(jnp.int32, (toks, toks), 0) > lax.broadcasted_iota(
        jnp.int32, (toks, toks), 1
    )
    ranks = jnp.dot(
        below.astype(F32).astype(BF), in_group.astype(BF), preferred_element_type=F32
    )
    rank = jnp.sum(ranks * in_group, axis=-1, keepdims=True).astype(jnp.int32)
    slot = group * block + rank
    slot_lane = lax.broadcasted_iota(jnp.int32, (toks, slots), 1)
    unpack = (slot == slot_lane).astype(F32)
    packing = unpack.T.astype(BF)
    step = min(slots, 128)
    for s in range(0, slots, step):
        pack[s : s + step, :] = jnp.dot(
            packing[s : s + step, :], xcat[...], preferred_element_type=F32
        ).astype(BF)
    rows_in[0, 0:block, :] = pack[0:block, :]

    pl.semaphore_wait(barrier, len(others))

    def remote(src, dst, s, r, dev):
        return pltpu.make_async_remote_copy(
            src_ref=src, dst_ref=dst, send_sem=s, recv_sem=r, device_id=dev, device_id_type=MESH
        )

    def place(d, pos):
        k, dd = d // per, d % per
        return rows_in.at[k, pl.ds(pos * seg + dd * block, block)]

    disp, core, xs, fwd, ret, pair, cross = {}, {}, {}, {}, {}, {}, {}
    for d in range(1, ep_count):
        disp[d] = remote(
            pack.at[pl.ds(d * block, block)], place(d, 0), disp_s.at[d], disp_r.at[d], peer[d]
        )
        disp[d].start()

    def spread(d):
        if d:
            disp[d].wait_recv()
        xs[d] = remote(place(d, 0), place(d, 1), x_s.at[d], x_r.at[d], across)
        xs[d].start()
        core[d] = remote(place(d, 0), place(d, 2), core_s.at[d], core_r.at[d], partner)
        core[d].start()

    def forward(d):
        xs[d].wait_recv()
        fwd[d] = remote(place(d, 1), place(d, 3), fwd_s.at[d], fwd_r.at[d], partner)
        fwd[d].start()

    def compute(k):
        for d in range(k * per, k * per + per):
            core[d].wait_recv()
            fwd[d].wait_recv()
        if k == 0:
            for c in w_copies:
                c.wait()
        total = tp_count * seg
        ends = lax.broadcasted_iota(jnp.int32, (total, 128), 1)
        mine = jnp.bitwise_and(ends, tp_count - 1) == me_t
        gates = jnp.sum(
            jnp.where(mine, rows_in[k, :, width:].astype(F32), 0.0), axis=-1, keepdims=True
        )
        f_tile = min(ff, 256)

        def up(j, carry):
            cols = pl.ds(pl.multiple_of(j * f_tile, f_tile), f_tile)
            rows = rows_in[k, :, :width]
            g = jnp.dot(rows, wg[:, cols], preferred_element_type=F32)
            u = jnp.dot(rows, wu[:, cols], preferred_element_type=F32)
            hid[:, cols] = (g / (1.0 + jnp.exp(-g)) * u).astype(BF)
            return carry

        lax.fori_loop(0, ff // f_tile, up, 0)
        d_tile = min(width, 512)

        def down(j, carry):
            cols = pl.ds(pl.multiple_of(j * d_tile, d_tile), d_tile)
            y = jnp.dot(hid[...], wd[:, cols], preferred_element_type=F32)
            part[k, :, cols] = (y * gates).astype(BF)
            return carry

        lax.fori_loop(0, width // d_tile, down, 0)
        pair[k] = remote(
            part.at[k, pl.ds(2 * seg, 2 * seg)], pair_in.at[k], pair_s.at[k], pair_r.at[k], partner
        )
        pair[k].start()

    def join_pair(k):
        pair[k].wait_recv()
        cross_out[k] = (
            part[k, seg : 2 * seg, :].astype(F32) + pair_in[k, seg:, :].astype(F32)
        ).astype(BF)
        cross[k] = remote(cross_out.at[k], cross_in.at[k], cross_s.at[k], cross_r.at[k], across)
        cross[k].start()

    def give_back(k):
        cross[k].wait_recv()
        done[k] = (
            part[k, 0:seg, :].astype(F32)
            + pair_in[k, 0:seg, :].astype(F32)
            + cross_in[k].astype(F32)
        ).astype(BF)
        for dd in range(per):
            d = k * per + dd
            if d == 0:
                back[0:block, :] = done[0, 0:block, :]
            else:
                ret[d] = remote(
                    done.at[k, pl.ds(dd * block, block)], back.at[pl.ds(d * block, block)],
                    ret_s.at[d], ret_r.at[d], peer[d],
                )
                ret[d].start()

    def each(f, k, lo=0, hi=None):
        for d in range(k * per + lo, k * per + (per if hi is None else hi)):
            f(d)

    half = per // 2
    each(spread, 0)
    each(forward, 0)
    each(spread, 1)
    compute(0)
    each(forward, 1)
    join_pair(0)
    compute(1)
    give_back(0)
    each(spread, 2)
    join_pair(1)
    each(forward, 2)
    give_back(1)
    compute(2)
    each(spread, 3, 0, half)
    join_pair(2)
    each(spread, 3, half)
    give_back(2)
    each(forward, 3)
    compute(3)
    join_pair(3)
    give_back(3)

    for d in range(1, ep_count):
        ret[d].wait_recv()
    out_ref[...] = jnp.dot(unpack.astype(BF), back[...], preferred_element_type=F32).astype(BF)
    for group_of in (disp, core, xs, fwd, pair, cross, ret):
        for c in group_of.values():
            c.wait_send()


def local(tokens, norm_gain, w_gate, w_up, w_down, routing, gate_weight):
    toks, width = tokens.shape
    ff = w_gate.shape[2]
    ep_count = lax.axis_size("ep")
    tp_count = lax.axis_size("tp")
    assert tp_count == 4 and ep_count % 8 == 0
    cap = toks // ep_count
    block = -(-cap // 16) * 16
    chunks = 4
    slots = ep_count * block
    seg = slots // chunks
    wide = width + 128
    vm = pl.BlockSpec(memory_space=pltpu.VMEM)
    hbm = pl.BlockSpec(memory_space=pl.ANY)
    dma = pltpu.SemaphoreType.DMA
    n_sem = [3] + [ep_count] * 8 + [chunks] * 4 + [ep_count] * 2
    return pl.pallas_call(
        functools.partial(kernel, ep_count, tp_count, block, chunks),
        out_shape=jax.ShapeDtypeStruct((toks, width), BF),
        in_specs=[vm] * 4 + [hbm] * 3,
        out_specs=vm,
        scratch_shapes=[
            pltpu.VMEM((width, ff), BF),
            pltpu.VMEM((width, ff), BF),
            pltpu.VMEM((ff, width), BF),
            pltpu.VMEM((toks, wide), BF),
            pltpu.VMEM((slots, wide), BF),
            pltpu.VMEM((chunks, tp_count * seg, wide), BF),
            pltpu.VMEM((tp_count * seg, ff), BF),
            pltpu.VMEM((chunks, tp_count * seg, width), BF),
            pltpu.VMEM((chunks, 2 * seg, width), BF),
            pltpu.VMEM((chunks, seg, width), BF),
            pltpu.VMEM((chunks, seg, width), BF),
            pltpu.VMEM((chunks, seg, width), BF),
            pltpu.VMEM((slots, width), BF),
        ] + [dma((n,)) for n in n_sem],
        compiler_params=pltpu.CompilerParams(
            collective_id=0, has_side_effects=True, vmem_limit_bytes=60 * 1024 * 1024
        ),
    )(tokens, norm_gain.reshape(1, width), routing, gate_weight, w_gate, w_up, w_down)


def solution(mesh):
    placed = (
        P(("ep", "tp"), None),
        P(),
        P(("ep", "tp"), None, None),
        P(("ep", "tp"), None, None),
        P(("ep", "tp"), None, None),
        P(("ep", "tp"), None),
        P(("ep", "tp"), None),
    )
    return jax.shard_map(
        local, mesh=mesh, in_specs=placed, out_specs=P(("ep", "tp"), None), check_vma=False
    )
```

profile of v0, /device:TPU:0, one launch (start us, length us, event | category | flops | bytes accessed | tf_op | source)
XLA Modules:
  0.0 60.1 jit_solution(3696284761307635575)
XLA Ops:
  0.0 1.4 %copy.8.route_ref = s32[128,2]{1,0:T(8,128)} copy(s32[128,2]{0,1:T(2,128)} %param.12) | data formatting | bytes 2048 | tf_op args[5]
  1.4 1.4 %copy.9.gate_ref = f32[128,2]{1,0:T(8,128)} copy(f32[128,2]{0,1:T(2,128)} %param.13) | data formatting | bytes 2048 | tf_op args[6]
  2.8 55.4 %shard_map.73 = bf16[128,2048]{1,0:T(8,128)(2,1)} custom-call(bf16[128,2048]{1,0:T(8,128)(2,1)} %tok_ref.1, f32[1,2048]{1,0:T(1,128)} %bitcast.1, s32[128,2]{1,0:T(8,128)} %copy.8.route_ref, f32[128,2]{1,0:T(8,128)} %copy.9.gate_ref, bf16[1,2048,512]{2,1,0:T(8,128)(2,1)} %wg_hbm.1, bf16[1,2048,512]{2,1,0:T(8,128)(2,1)} %wu_hbm.1, bf16[1,512,2048]{2,1,0:T(8,128)(2,1)} %wd_hbm.1), custom_call_target="tpu_custom_call" | custom-call | tf_op jit(solution)/shard_map/pallas_call | solution.py:234
  58.2 1.9 %copy.11 = bf16[128,2048]{1,0:T(8,128)(2,1)} copy(bf16[128,2048]{1,0:T(8,128)(2,1)} %shard_map.73) | data formatting | bytes 1048576
where the time goes:
time: 60.8 us; the launch traced here: 60.1 us
  Pallas kernels  55.4 us (91%)
  local copies, waits for them, and re-layouts  4.7 us (8%)
    pallas_call x1, Pallas kernels, local(): pl.pallas_call(functools.partial(kernel, ep_count, tp_count, block, chunk...  55.4 us
    unnamed x3, local copies, waits for them, and re-layouts  4.7 us

commit v1 on v0

v1 whole, which is shorter than its diff:
```python
import functools
import jax
import jax.numpy as jnp
from jax import lax
from jax.experimental import pallas as pl
from jax.experimental.pallas import tpu as pltpu
from jax.sharding import PartitionSpec as P

BF = jnp.bfloat16
F32 = jnp.float32
MESH = pl.DeviceIdType.MESH

CHUNKS = ((0, 1), (2, 3), (4, 5), (6, 7))
ORDER = (
    "S0 S1 F0 S2",
    "S3 F1 S4 C0",
    "F2 F3 S5 C1",
    "F4 S6 F5 S7",
    "C2 J2 J1 F6",
    "F7 C3 G4 G5",
    "J3 J0 G2 G3",
    "G6 G7",
)
DIRECT = 2
RDIRECT = 2
SENDS = (
    "P1 X1 P2 P3",
    "P4 P5 P6 P7",
)


def flip(index, bits):
    unit = 1
    while unit <= bits:
        if bits & unit:
            index = index + unit - 2 * unit * lax.rem(lax.div(index, unit), 2)
        unit *= 2
    return index


def kernel(
    ep_count, tp_count, block,
    tok_ref, gain_ref, route_ref, gate_ref, wg_hbm, wu_hbm, wd_hbm, out_ref,
    wg, wu, wd, normed, pack, rows_in, hid, part, pair_in, cross_out, cross_in, done, back, back_x,
    w_sem, disp_s, disp_r, core_s, core_r, x_s, x_r, fwd_s, fwd_r,
    pair_s, pair_r, cross_s, cross_r, ret_s, ret_r, rx_s, rx_r,
):
    toks, width = tok_ref.shape
    ff = wg.shape[1]
    slots = ep_count * block
    unit = ep_count // 8
    me_e = lax.axis_index("ep")
    me_t = lax.axis_index("tp")
    partner = {"tp": flip(me_t, 1)}
    across = {"tp": flip(me_t, 2)}
    peer = [{"ep": flip(me_e, d)} for d in range(ep_count)]
    direct, r_direct = DIRECT * unit, RDIRECT * unit
    far_side = [across] + [
        {"ep": flip(me_e, d), "tp": flip(me_t, 2)} for d in range(1, max(direct, r_direct))
    ]

    w_copies = [
        pltpu.make_async_copy(src.at[0], dst, w_sem.at[i])
        for i, (src, dst) in enumerate(((wg_hbm, wg), (wu_hbm, wu), (wd_hbm, wd)))
    ]
    barrier = pltpu.get_barrier_semaphore()
    others = peer[1:] + [partner] + far_side
    for dev in others:
        pl.semaphore_signal(barrier, inc=1, device_id=dev, device_id_type=MESH)
    for c in w_copies:
        c.start()

    values = tok_ref[...].astype(F32)
    scale = lax.rsqrt(jnp.mean(values * values, axis=-1, keepdims=True) + 1e-06)
    normed[...] = (values * scale * gain_ref[...]).astype(BF)

    shift = tp_count.bit_length() - 1
    group = jnp.bitwise_xor(jnp.right_shift(route_ref[0:1, :], shift), me_e)
    in_group = (group == lax.broadcasted_iota(jnp.int32, (ep_count, toks), 0)).astype(F32)
    before = lax.broadcasted_iota(jnp.int32, (toks, toks), 0) < lax.broadcasted_iota(
        jnp.int32, (toks, toks), 1
    )
    ranks = jnp.dot(
        in_group.astype(BF), before.astype(F32).astype(BF), preferred_element_type=F32
    )
    rank = jnp.sum(ranks * in_group, axis=0, keepdims=True).astype(jnp.int32)
    slot = group * block + rank
    packing = slot == lax.broadcasted_iota(jnp.int32, (slots, toks), 0)
    packs = packing.astype(F32).astype(BF)
    step = min(slots, 128)
    for s in range(0, slots, step):
        pack[s : s + step, :width] = jnp.dot(
            packs[s : s + step, :], normed[...], preferred_element_type=F32
        ).astype(BF)
    lane = lax.broadcasted_iota(jnp.int32, (slots, 128), 1)
    weight = jnp.zeros((slots, 128), F32)
    for j in range(tp_count):
        one = jnp.zeros((1, toks), F32)
        for k in range(route_ref.shape[0]):
            hit = jnp.bitwise_and(route_ref[k : k + 1, :], tp_count - 1) == j
            one = one + jnp.where(hit, gate_ref[k : k + 1, :], 0.0)
        picked = jnp.sum(jnp.where(packing, one, 0.0), axis=-1, keepdims=True)
        weight = jnp.where(jnp.bitwise_and(lane, tp_count - 1) == j, picked, weight)
    hi = weight.astype(BF).astype(F32)
    mid = (weight - hi).astype(BF).astype(F32)
    low = weight - hi - mid
    tail = jnp.where(lane < tp_count, hi, jnp.where(lane < 2 * tp_count, mid, low))
    pack[:, width:] = jnp.where(lane < 3 * tp_count, tail, 0.0).astype(BF)

    def remote(src, dst, s, r, dev):
        return pltpu.make_async_remote_copy(
            src_ref=src, dst_ref=dst, send_sem=s, recv_sem=r, device_id=dev, device_id_type=MESH
        )

    chunk_of = {}
    first, count, base = [], [], []
    for k, units in enumerate(CHUNKS):
        first.append(units[0] * unit)
        count.append(len(units) * unit)
        base.append(units[0] * unit * block)
        for d in range(first[k], first[k] + count[k]):
            chunk_of[d] = k

    def place(d, pos):
        k = chunk_of[d]
        seg = count[k] * block
        return rows_in.at[pl.ds(tp_count * base[k] + pos * seg + (d - first[k]) * block, block)]

    rows_in[0:block, :] = pack[0:block, :]
    pl.semaphore_wait(barrier, len(others))

    disp, core, xs, fwd, ret, ret_x, pair, cross = ({} for _ in range(8))

    def send_peer(d):
        disp[d] = remote(
            pack.at[pl.ds(d * block, block)], place(d, 0), disp_s.at[d], disp_r.at[d], peer[d]
        )
        disp[d].start()

    def send_across(d, dev):
        src = pack.at[pl.ds(d * block, block)] if d < direct else place(d, 0)
        xs[d] = remote(src, place(d, 1), x_s.at[d], x_r.at[d], dev)
        xs[d].start()

    def send_core(d):
        core[d] = remote(place(d, 0), place(d, 2), core_s.at[d], core_r.at[d], partner)
        core[d].start()

    send_across(0, across)
    send_core(0)
    for d in range(1, unit):
        send_peer(d)
        send_across(d, far_side[d])
    for word in " ".join(SENDS).split():
        i = int(word[1:])
        for d in range(i * unit, i * unit + unit):
            if word[0] == "P":
                send_peer(d)
            else:
                send_across(d, far_side[d])

    def spread(i):
        for d in range(i * unit, i * unit + unit):
            if d > 0:
                disp[d].wait_recv()
                if d >= direct:
                    send_across(d, across)
                send_core(d)

    def forward(i):
        for d in range(i * unit, i * unit + unit):
            xs[d].wait_recv()
            fwd[d] = remote(place(d, 1), place(d, 3), fwd_s.at[d], fwd_r.at[d], partner)
            fwd[d].start()

    def compute(k):
        for d in range(first[k], first[k] + count[k]):
            core[d].wait_recv()
            fwd[d].wait_recv()
        if k == 0:
            for c in w_copies:
                c.wait()
        seg = count[k] * block
        total = tp_count * seg
        mine = pl.ds(tp_count * base[k], total)
        ends = lax.broadcasted_iota(jnp.int32, (total, 128), 1)
        own = jnp.bitwise_and(ends, tp_count - 1) == me_t
        gates = jnp.sum(
            jnp.where(own, rows_in[mine, width:].astype(F32), 0.0), axis=-1, keepdims=True
        )
        f_tile = min(ff, 256)
        for j in range(0, ff, f_tile):
            rows = rows_in[mine, :width]
            g = jnp.dot(rows, wg[:, j : j + f_tile], preferred_element_type=F32)
            u = jnp.dot(rows, wu[:, j : j + f_tile], preferred_element_type=F32)
            hid[0:total, j : j + f_tile] = (g / (1.0 + jnp.exp(-g)) * u).astype(BF)
        d_tile = min(width, 512)
        for j in range(0, width, d_tile):
            y = jnp.dot(hid[0:total, :], wd[:, j : j + d_tile], preferred_element_type=F32)
            part[mine, j : j + d_tile] = (y * gates).astype(BF)
        pair[k] = remote(
            part.at[pl.ds(tp_count * base[k] + 2 * seg, 2 * seg)],
            pair_in.at[pl.ds(2 * base[k], 2 * seg)], pair_s.at[k], pair_r.at[k], partner,
        )
        pair[k].start()

    def give_block(d):
        ret[d] = remote(
            done.at[pl.ds(d * block, block)], back.at[pl.ds(d * block, block)],
            ret_s.at[d], ret_r.at[d], peer[d],
        )
        ret[d].start()

    def join(k):
        pair[k].wait_recv()
        seg = count[k] * block
        b, p = base[k], tp_count * base[k]
        cross_out[b : b + seg, :] = (
            part[p + seg : p + 2 * seg, :].astype(F32)
            + pair_in[2 * b + seg : 2 * b + 2 * seg, :].astype(F32)
        ).astype(BF)
        if first[k] >= r_direct:
            for d in range(first[k], first[k] + count[k]):
                cross[d] = remote(
                    cross_out.at[pl.ds(d * block, block)], cross_in.at[pl.ds(d * block, block)],
                    cross_s.at[d], cross_r.at[d], across,
                )
                cross[d].start()
            return
        for d in range(first[k], first[k] + count[k]):
            ret_x[d] = remote(
                cross_out.at[pl.ds(d * block, block)], back_x.at[pl.ds(d * block, block)],
                rx_s.at[d], rx_r.at[d], far_side[d],
            )
            ret_x[d].start()
        total = (
            part[p : p + seg, :].astype(F32) + pair_in[2 * b : 2 * b + seg, :].astype(F32)
        ).astype(BF)
        done[b : b + seg, :] = total
        for d in range(first[k], first[k] + count[k]):
            if d == 0:
                back[0:block, :] = total[0:block, :]
            else:
                give_block(d)

    def give(i):
        for d in range(i * unit, i * unit + unit):
            cross[d].wait_recv()
            k = chunk_of[d]
            b, p = d * block, tp_count * base[k] + (d - first[k]) * block
            q = 2 * base[k] + (d - first[k]) * block
            done[b : b + block, :] = (
                part[p : p + block, :].astype(F32)
                + pair_in[q : q + block, :].astype(F32)
                + cross_in[b : b + block, :].astype(F32)
            ).astype(BF)
            give_block(d)

    step_of = {"S": spread, "F": forward, "C": compute, "J": join, "G": give}
    for word in " ".join(ORDER).split():
        step_of[word[0]](int(word[1:]))

    for d in sorted(ret):
        ret[d].wait_recv()
    for d in sorted(ret_x):
        ret_x[d].wait_recv()
    unpack = packing.astype(F32).T.astype(BF)
    total = jnp.dot(unpack, back[...], preferred_element_type=F32)
    total = total + jnp.dot(
        unpack[:, : r_direct * block], back_x[...], preferred_element_type=F32
    )
    out_ref[...] = total.astype(BF)
    for group_of in (disp, core, xs, fwd, pair, cross, ret, ret_x):
        for c in group_of.values():
            c.wait_send()


def local(tokens, norm_gain, w_gate, w_up, w_down, routing, gate_weight):
    toks, width = tokens.shape
    ff = w_gate.shape[2]
    ep_count = lax.axis_size("ep")
    tp_count = lax.axis_size("tp")
    assert tp_count == 4 and ep_count % 8 == 0
    cap = toks // ep_count
    block = -(-cap // 16) * 16
    slots = ep_count * block
    wide = width + 128
    most = tp_count * block * (ep_count // 8) * max(len(units) for units in CHUNKS)
    vm = pl.BlockSpec(memory_space=pltpu.VMEM)
    hbm = pl.BlockSpec(memory_space=pl.ANY)
    dma = pltpu.SemaphoreType.DMA
    n_sem = [3] + [ep_count] * 8 + [len(CHUNKS)] * 2 + [ep_count] * 6
    return pl.pallas_call(
        functools.partial(kernel, ep_count, tp_count, block),
        out_shape=jax.ShapeDtypeStruct((toks, width), BF),
        in_specs=[vm] * 4 + [hbm] * 3,
        out_specs=vm,
        scratch_shapes=[
            pltpu.VMEM((width, ff), BF),
            pltpu.VMEM((width, ff), BF),
            pltpu.VMEM((ff, width), BF),
            pltpu.VMEM((toks, width), BF),
            pltpu.VMEM((slots, wide), BF),
            pltpu.VMEM((tp_count * slots, wide), BF),
            pltpu.VMEM((most, ff), BF),
            pltpu.VMEM((tp_count * slots, width), BF),
            pltpu.VMEM((2 * slots, width), BF),
            pltpu.VMEM((slots, width), BF),
            pltpu.VMEM((slots, width), BF),
            pltpu.VMEM((slots, width), BF),
            pltpu.VMEM((slots, width), BF),
            pltpu.VMEM((RDIRECT * slots // 8, width), BF),
        ] + [dma((n,)) for n in n_sem],
        compiler_params=pltpu.CompilerParams(
            collective_id=0, has_side_effects=True, vmem_limit_bytes=60 * 1024 * 1024
        ),
    )(tokens, norm_gain.reshape(1, width), routing.T, gate_weight.T, w_gate, w_up, w_down)


def solution(mesh):
    placed = (
        P(("ep", "tp"), None),
        P(),
        P(("ep", "tp"), None, None),
        P(("ep", "tp"), None, None),
        P(("ep", "tp"), None, None),
        P(("ep", "tp"), None),
        P(("ep", "tp"), None),
    )
    return jax.shard_map(
        local, mesh=mesh, in_specs=placed, out_specs=P(("ep", "tp"), None), check_vma=False
    )
```

time: 60.8 us -> 46 us (0.76)
  Pallas kernels: 55.4 us -> 43.9 us
  local copies, waits for them, and re-layouts: 4.7 us -> 1.88 us
    pallas_call x1, Pallas kernels: 55.4 us -> 43.9 us  [local(): pl.pallas_call(functools.partial(kernel, ep_count, tp_count, block), out_...]
    unnamed x3 -> x1, local copies, waits for them, and re-layouts: 4.7 us -> 1.88 us
where the time goes in v1:
time: 46 us; the launch traced here: 45.8 us
  Pallas kernels  43.9 us (95%)
  local copies, waits for them, and re-layouts  1.88 us (4%)
    pallas_call x1, Pallas kernels, local(): pl.pallas_call(functools.partial(kernel, ep_count, tp_count, block), out_...  43.9 us
    unnamed x1, local copies, waits for them, and re-layouts  1.88 us

profile of v1, /device:TPU:0, one launch (start us, length us, event | category | flops | bytes accessed | tf_op | source)
XLA Modules:
  0.0 45.8 jit_solution(16788285493455157691)
XLA Ops:
  0.0 43.9 %shard_map.73 = bf16[128,2048]{1,0:T(8,128)(2,1)} custom-call(bf16[128,2048]{1,0:T(8,128)(2,1)} %tok_ref.1, f32[1,2048]{1,0:T(1,128)} %bitcast.3, s32[2,128]{1,0:T(2,128)} %bitcast.4, f32[2,128]{1,0:T(2,128)} %bitcast.5, bf16[1,2048,512]{2,1,0:T(8,128)(2,1)} %wg_hbm.1, bf16[1,2048,512]{2,1,0:T(8,128)(2,1)} %wu_hbm.1, bf16[1,512,2048]{2,1,0:T(8,128)(2,1)} %wd_hbm.1), custom_call_target="tpu_custom_call" | custom-call | tf_op jit(solution)/shard_map/pallas_call | solution.py:293
  43.9 1.9 %copy.9 = bf16[128,2048]{1,0:T(8,128)(2,1)} copy(bf16[128,2048]{1,0:T(8,128)(2,1)} %shard_map.73) | data formatting | bytes 1048576

commit v2 on v1

--- a/solution.py
+++ b/solution.py
@@ -10,22 +10,23 @@
 F32 = jnp.float32
 MESH = pl.DeviceIdType.MESH
 
-CHUNKS = ((0, 1), (2, 3), (4, 5), (6, 7))
+CHUNKS = ((0, 1), (2, 3), (4,), (5,), (6,), (7,))
 ORDER = (
-    "S0 S1 F0 S2",
-    "S3 F1 S4 C0",
-    "F2 F3 S5 C1",
-    "F4 S6 F5 S7",
-    "C2 J2 J1 F6",
-    "F7 C3 G4 G5",
-    "J3 J0 G2 G3",
-    "G6 G7",
+    "S0 F0 S4 S2",
+    "S3 F4 S5 C2",
+    "F2 F3 S7 F5",
+    "C1 S1 J2 F1",
+    "C3 S6 F7 J3",
+    "C5 G4 J1 F6",
+    "C4 J5 G5 C0",
+    "G3 J4 G7 J0",
+    "G6 G2",
 )
 DIRECT = 2
 RDIRECT = 2
 SENDS = (
-    "P1 X1 P2 P3",
-    "P4 P5 P6 P7",
+    "P2 P4 P1 P3",
+    "P5 P7 X1 P6",
 )
 
 
@@ -177,7 +178,7 @@
         for d in range(first[k], first[k] + count[k]):
             core[d].wait_recv()
             fwd[d].wait_recv()
-        if k == 0:
+        if not pair:
             for c in w_copies:
                 c.wait()
         seg = count[k] * block

time: 46 us -> 44.9 us (0.976)
  Pallas kernels: 43.9 us -> 42.8 us
    pallas_call x1, Pallas kernels: 43.9 us -> 42.8 us  [local(): pl.pallas_call(functools.partial(kernel, ep_count, tp_count, block), out_...]
where the time goes in v2:
time: 44.9 us; the launch traced here: 44.7 us
  Pallas kernels  42.8 us (95%)
  local copies, waits for them, and re-layouts  1.88 us (4%)
    pallas_call x1, Pallas kernels, local(): pl.pallas_call(functools.partial(kernel, ep_count, tp_count, block), out_...  42.8 us
    unnamed x1, local copies, waits for them, and re-layouts  1.88 us

profile of v2, /device:TPU:0, one launch (start us, length us, event | category | flops | bytes accessed | tf_op | source)
XLA Modules:
  0.0 44.7 jit_solution(14205122041912234318)
XLA Ops:
  0.0 42.8 %shard_map.73 = bf16[128,2048]{1,0:T(8,128)(2,1)} custom-call(bf16[128,2048]{1,0:T(8,128)(2,1)} %tok_ref.1, f32[1,2048]{1,0:T(1,128)} %bitcast.3, s32[2,128]{1,0:T(2,128)} %bitcast.4, f32[2,128]{1,0:T(2,128)} %bitcast.5, bf16[1,2048,512]{2,1,0:T(8,128)(2,1)} %wg_hbm.1, bf16[1,2048,512]{2,1,0:T(8,128)(2,1)} %wu_hbm.1, bf16[1,512,2048]{2,1,0:T(8,128)(2,1)} %wd_hbm.1), custom_call_target="tpu_custom_call" | custom-call | tf_op jit(solution)/shard_map/pallas_call | solution.py:294
  42.8 1.9 %copy.9 = bf16[128,2048]{1,0:T(8,128)(2,1)} copy(bf16[128,2048]{1,0:T(8,128)(2,1)} %shard_map.73) | data formatting | bytes 1048576

commit v3 on v2

--- a/solution.py
+++ b/solution.py
@@ -19,7 +19,7 @@
     "C3 S6 F7 J3",
     "C5 G4 J1 F6",
     "C4 J5 G5 C0",
-    "G3 J4 G7 J0",
+    "G3 J4 J0 G7",
     "G6 G2",
 )
 DIRECT = 2

time: 44.9 us -> 45.3 us (level)
  no operation moved by 1% of the time
where the time goes in v3:
time: 45.3 us; the launch traced here: 45.1 us
  Pallas kernels  43.2 us (95%)
  local copies, waits for them, and re-layouts  1.88 us (4%)
    pallas_call x1, Pallas kernels, local(): pl.pallas_call(functools.partial(kernel, ep_count, tp_count, block), out_...  43.2 us
    unnamed x1, local copies, waits for them, and re-layouts  1.88 us

profile of v3, /device:TPU:0, one launch (start us, length us, event | category | flops | bytes accessed | tf_op | source)
XLA Modules:
  0.0 45.1 jit_solution(5081426254158101641)
XLA Ops:
  0.0 43.2 %shard_map.73 = bf16[128,2048]{1,0:T(8,128)(2,1)} custom-call(bf16[128,2048]{1,0:T(8,128)(2,1)} %tok_ref.1, f32[1,2048]{1,0:T(1,128)} %bitcast.3, s32[2,128]{1,0:T(2,128)} %bitcast.4, f32[2,128]{1,0:T(2,128)} %bitcast.5, bf16[1,2048,512]{2,1,0:T(8,128)(2,1)} %wg_hbm.1, bf16[1,2048,512]{2,1,0:T(8,128)(2,1)} %wu_hbm.1, bf16[1,512,2048]{2,1,0:T(8,128)(2,1)} %wd_hbm.1), custom_call_target="tpu_custom_call" | custom-call | tf_op jit(solution)/shard_map/pallas_call | solution.py:294
  43.2 1.9 %copy.9 = bf16[128,2048]{1,0:T(8,128)(2,1)} copy(bf16[128,2048]{1,0:T(8,128)(2,1)} %shard_map.73) | data formatting | bytes 1048576
